TPU v7x, 32 devices: a whole 2x2x4 slice. The times are simulated.
32 devices in a mesh: sp: 8 (over z, core), tp: 4 (over y, x).
Axes of the slice: x: 2, y: 2, z: 4, core: 2. Of those that a mesh axis runs over, the one named last changes fastest.
Arguments:
- residual_in: bfloat16 [2048, 2048], P('sp'), may hold values from -6 to 6
- queries: bfloat16 [2048, 2048], P('sp', 'tp'), may hold values from -6 to 4
- keys: bfloat16 [2048, 2048], P('sp', 'tp'), may hold values from -4 to 5.2
- values: bfloat16 [2048, 2048], P('sp', 'tp'), may hold values from -9.5 to 9.5
- out_weight: bfloat16 [2048, 2048], P('tp'), may hold values from -0.125 to 0.125
- norm_gain: float32 [2048], replicated, may hold values from 0.1 to 1.9
- expert_routes: int32 [2048, 2], P('sp'), may hold values from 0 to 7, all different within a row; in each aligned block of 256 rows (0 to 255, 256 to 511, ...) at most 128 rows name the same one
- route_scores: float32 [2048, 2], P('sp'), may hold values from -6 to 6
- gate_weight: bfloat16 [8, 2048, 4096], P('sp', None, 'tp'), may hold values from -0.125 to 0.125
- up_weight: bfloat16 [8, 2048, 4096], P('sp', None, 'tp'), may hold values from -0.125 to 0.125
- down_weight: bfloat16 [8, 4096, 2048], P('sp', 'tp'), may hold values from -0.09375 to 0.09375
Outputs:
- layer_out: bfloat16 [2048, 2048], P('sp', 'tp')
Inputs may be any that keep to these rules, and one draw needn't show every extreme that they name: `expert_routes`: each row names 2 different experts; among the 256 rows of one index of sp no expert is named more than 128 times, and in every draw some such block names some expert exactly 128 times.
All inputs are finite; a program needn't handle non-finite values.
Results may differ from a plain program's by a relative error of at most 0.015.
Values may be sent and summed in bfloat16 or wider, within the bound.
A program may use at most 64 MiB of HBM per device.

v0:
```python
import jax
import jax.numpy as jnp
from jax import lax
from jax.sharding import PartitionSpec as P

HD = 64
epsilon = 1e-06


def attend(queries, query_start, keys_all, values_all):
    row_count = queries.shape[0]
    total_len = keys_all.shape[0]
    head_count = queries.shape[1] // HD
    span = min(512, total_len)
    scale = HD ** (-0.5)
    query_heads = queries.reshape(row_count, head_count, HD)
    query_pos = query_start + lax.iota(jnp.int32, row_count)
    block_count = (query_start + row_count - 1 + span - 1) // span

    def one_block(step_index, state_pair):
        accumulated, kept_log = state_pair
        key_start = (block_count - 1 - step_index) * span
        key_block = lax.dynamic_slice_in_dim(keys_all, key_start, span, 0).reshape(
            span, head_count, HD
        )
        value_block = lax.dynamic_slice_in_dim(values_all, key_start, span, 0).reshape(
            span, head_count, HD
        )
        scores = (
            jnp.einsum("qhc,khc->hqk", query_heads, key_block, preferred_element_type=jnp.float32)
            * scale
        )
        key_pos = key_start + lax.iota(jnp.int32, span)
        causal = key_pos[None, :] < query_pos[:, None]
        log_keep = jnp.where(causal, jax.nn.log_sigmoid(-scores), 0.0)
        between = lax.cumsum(log_keep, axis=2, reverse=True) - log_keep + kept_log[:, :, None]
        weights = jnp.where(causal, jnp.exp(jax.nn.log_sigmoid(scores) + between), 0.0).astype(
            jnp.bfloat16
        )
        accumulated = accumulated + jnp.einsum(
            "hqk,khc->qhc", weights, value_block, preferred_element_type=jnp.float32
        )
        return (accumulated, kept_log + jnp.sum(log_keep, axis=2))

    start_pair = (
        jnp.zeros((row_count, head_count, HD), jnp.float32),
        jnp.zeros((head_count, row_count), jnp.float32),
    )
    accumulated, kept_log = lax.fori_loop(0, block_count, one_block, start_pair)
    return accumulated.reshape(row_count, head_count * HD).astype(jnp.bfloat16)


def route_targets(routes, experts, capacity):
    flat_routes = routes.reshape(-1)
    onehot = (flat_routes[:, None] == lax.iota(jnp.int32, experts)[None, :]).astype(jnp.int32)
    before = jnp.cumsum(onehot, axis=0) - onehot
    return flat_routes * capacity + jnp.sum(before * onehot, axis=1)


def shards(
    residual_in,
    queries,
    keys,
    values,
    out_weight,
    norm_gain,
    expert_routes,
    route_scores,
    gate_weight,
    up_weight,
    down_weight,
):
    row_count = residual_in.shape[0]
    width = residual_in.shape[1]
    row_start = lax.axis_index("sp") * row_count
    keys_all, values_all = (
        lax.all_gather(keys, "sp", axis=0, tiled=True),
        lax.all_gather(values, "sp", axis=0, tiled=True),
    )
    mixed_heads = attend(queries, row_start, keys_all, values_all)
    partial_value = jnp.dot(mixed_heads, out_weight, preferred_element_type=jnp.float32).astype(
        jnp.bfloat16
    )
    attended = lax.psum(partial_value, "tp").astype(jnp.float32).astype(jnp.bfloat16)
    stream = (residual_in.astype(jnp.float32) + attended.astype(jnp.float32)).astype(jnp.bfloat16)
    stream_wide = stream.astype(jnp.float32)
    normed = (
        stream_wide
        * lax.rsqrt(jnp.mean(stream_wide * stream_wide, axis=1, keepdims=True) + epsilon)
        * norm_gain
    ).astype(jnp.bfloat16)
    experts = lax.axis_size("sp")
    capacity = 4 * row_count // experts
    top_count = expert_routes.shape[1]
    targets = route_targets(expert_routes, experts, capacity)
    owners = lax.iota(jnp.int32, row_count * top_count) // top_count
    slot_owner = jnp.full((experts * capacity,), row_count, jnp.int32).at[targets].set(owners)
    padded = jnp.concatenate([normed, jnp.zeros((1, width), jnp.bfloat16)], axis=0)
    outgoing = padded[slot_owner].reshape(experts, capacity, width)
    col_count = width // lax.axis_size("tp")
    column_start = lax.axis_index("tp") * col_count
    own_part = lax.dynamic_slice_in_dim(outgoing, column_start, col_count, 2)
    arrived = lax.all_to_all(own_part, "sp", split_axis=0, concat_axis=0, tiled=True)
    arrived = lax.all_gather(arrived, "tp", axis=2, tiled=True)
    slot_rows = arrived.reshape(-1, width)
    gate_act = jnp.dot(slot_rows, gate_weight[0], preferred_element_type=jnp.float32)
    up_act = jnp.dot(slot_rows, up_weight[0], preferred_element_type=jnp.float32)
    hidden = (jax.nn.silu(gate_act) * up_act).astype(jnp.bfloat16)
    expert_part = (
        jnp.dot(hidden, down_weight[0], preferred_element_type=jnp.float32)
        .astype(jnp.bfloat16)
        .reshape(arrived.shape)
    )
    summed = (
        lax.psum_scatter(expert_part, "tp", scatter_dimension=2, tiled=True)
        .astype(jnp.float32)
        .astype(jnp.bfloat16)
    )
    returned = lax.all_to_all(summed, "sp", split_axis=0, concat_axis=0, tiled=True)
    results = returned.reshape(experts * capacity, col_count)
    picked = results[targets].astype(jnp.float32).reshape(row_count, top_count, col_count)
    shares = jax.nn.sigmoid(route_scores - route_scores[:, ::-1])
    combined = jnp.sum(picked * shares[:, :, None], axis=1)
    own_columns = lax.dynamic_slice_in_dim(stream_wide, column_start, col_count, 1)
    return (own_columns + combined).astype(jnp.bfloat16)


def solution(mesh):
    in_specs = (
        P("sp", None),
        P("sp", "tp"),
        P("sp", "tp"),
        P("sp", "tp"),
        P("tp", None),
        P(),
        P("sp", None),
        P("sp", None),
        P("sp", None, "tp"),
        P("sp", None, "tp"),
        P("sp", "tp", None),
    )
    out_specs = P("sp", "tp")
    return jax.shard_map(shards, mesh=mesh, in_specs=in_specs, out_specs=out_specs, check_vma=False)
```

profile of v0, /device:TPU:0, one launch (start us, length us, event | category | flops | bytes accessed | tf_op | source)
XLA Modules:
  0.0 431.7 jit_solution(17356037483601882176)
XLA Ops:
  6.5 1.9 copy.22
  8.6 1.8 copy.23
  10.4 1.1 copy.24
  11.5 30.8 %all-gather.4.cloned.1.call-done = bf16[2048,512]{0,1:T(8,128)(2,1)} async-done(((bf16[256,512]{0,1:T(8,128)(2,1)}), bf16[2048,512]{0,1:T(8,128)(2,1)}) %all-gather.4.cloned.1.call-update) | async-done | bytes 2097168 | tf_op jit(solution)/shard_map/all_gather | solution.py:78
  42.3 31.2 %all-gather.6.cloned.1.call-done = bf16[2048,512]{0,1:T(8,128)(2,1)} async-done(((bf16[256,512]{0,1:T(8,128)(2,1)}), bf16[2048,512]{0,1:T(8,128)(2,1)}) %all-gather.6.cloned.1.call-update) | async-done | bytes 2097168 | tf_op jit(solution)/shard_map/all_gather | solution.py:77
  73.6 23.8 %while.15 = (s32[]{:T(128)}, f32[256,8,64]{0,2,1:T(8,128)S(1)}, f32[8,256]{1,0:T(8,128)S(1)}, s32[]{:T(128)}, s32[]{:T(128)}, /*index=5*/bf16[2048,512]{0,1:T(8,...) while((s32[]{:T(128)}, f32[256,8,64]{0,2,1:T(8,128)S(1)}, ...), condition=%wide.region_4.5_spmd.clone, body=%wide.region_0.4_spmd.clone.sunk | while | flops 436501248 | bytes 51206344 | solution.py:49
  73.6 1.3 constant_dynamic-slice_fusion.4
  75.1 3.6 fusion.64
  78.7 10.1 %fusion.65 = f32[8,256,4,128]{1,0,3,2:T(8,128)S(1)} fusion(f32[8,256,4,128]{1,3,2,0:T(8,128)S(1)} %bitcast.101), kind=kOutput, calls=%fused_computation.22.clone.1 | output fusion | flops 133169152 | bytes 8388608 | tf_op jit(solution)/shard_map/reduce-window.6
  89.2 1.4 copy.35
  90.6 6.3 %fusion.67 = bf16[8,256,512]{1,2,0:T(8,128)(2,1)S(1)} fusion(f32[8,256,4,128]{1,3,2,0:T(8,128)S(1)} %copy.35, f32[8,512,256]{2,1,0:T(8,128)S(1)} %get-tuple-element.219, f32[8,256]{1,0:T(8,128)S(1)} %get-tuple-element.236, pred[256,512]{0,1:T(8,128)(4,1)S(1)} %broadcast_compare_fusion.2), kind=kLoop, calls=%fused_computation.10.clone.1 | loop fusion | flops 23068672 | bytes 10625024 | tf_op jit(solution)/shard_map/while/body/convert_element_type | solution.py:37
  96.9 0.5 fusion.68
  97.5 1.8 convolution_convert_fusion
  100.1 1.1 reduce-window.24
  101.6 2.6 scatter_custom_fusion
  104.3 117.7 %all-reduce.3.cloned.1.call-done = bf16[256,2048]{1,0:T(8,128)(2,1)} async-done(((bf16[256,2048]{1,0:T(8,128)(2,1)}), bf16[256,2048]{1,0:T(8,128)(2,1)}) %all-reduce.3.cloned.1.call-update) | async-done | bytes 1048592 | tf_op jit(solution)/shard_map/psum | solution.py:84
  222.0 3.0 fusion.30
  225.0 0.5 multiply_convert_fusion.1
  225.6 6.0 %gather_fusion = bf16[1024,2048]{1,0:T(8,128)(2,1)} fusion(bf16[257,2048]{1,0:T(8,128)(2,1)S(1)} %concatenate.3, s32[1024]{0:T(1024)S(1)} %fusion.34), kind=kCustom, calls=%fused_computation | custom fusion | bytes 8392704 | tf_op jit(solution)/shard_map/gather | solution.py:99
  231.6 1.3 constant_dynamic-slice_fusion.2
  233.0 31.1 %all_to_all.10 = bf16[8,128,512]{2,1,0:T(8,128)(2,1)} all-to-all(bf16[8,128,512]{2,1,0:T(8,128)(2,1)S(1)} %constant_dynamic-slice_fusion.2), channel_id=1, replica_groups=mesh['sp'=8,'tp'=4] {'sp'}, dimensions={0} | all-to-all | bytes 2097152 | tf_op jit(solution)/shard_map/all_to_all | solution.py:103
  264.1 50.5 %all-gather.8.cloned.1.call-done = bf16[8,128,2048]{2,1,0:T(8,128)(2,1)} async-done(((bf16[8,128,512]{2,1,0:T(8,128)(2,1)}), bf16[8,128,2048]{2,1,0:T(8,128)(2,1)}) %all-gather.8.cloned.1.call-update) | async-done | bytes 4194320 | tf_op jit(solution)/shard_map/all_gather | solution.py:104
  314.6 7.6 %fusion.21 = f32[1024,1024]{1,0:T(8,128)S(1)} fusion(bf16[1024,2048]{1,0:T(8,128)(2,1)} %bitcast.112, bf16[1,2048,1024]{2,1,0:T(8,128)(2,1)} %param.22), kind=kOutput, calls=%fused_computation.37 | convolution fusion | flops 4294967296 | bytes 12582912 | tf_op jit(solution)/shard_map/dot_general | solution.py:107
  322.3 5.4 %multiply_convert_fusion = bf16[1024,1024]{1,0:T(8,128)(2,1)S(1)} fusion(f32[1024,1024]{1,0:T(8,128)S(1)} %fusion.21, bf16[1024,2048]{1,0:T(8,128)(2,1)S(1)} %bitcast.113, bf16[1,2048,1024]{2,1,0:T(8,128)(2,1)S(1)} %copy-done.6), kind=kOutput, calls=%fused_computation.41 | convolution fusion | flops 4301258752 | bytes 14680064 | tf_op jit(solution)/shard_map/dot_general | solution.py:106
  327.7 6.1 %fusion.25 = bf16[1024,2048]{1,0:T(8,128)(2,1)} fusion(bf16[1024,1024]{1,0:T(8,128)(2,1)S(1)} %multiply_convert_fusion, bf16[1,1024,2048]{2,1,0:T(8,128)(2,1)S(1)} %copy-done.7), kind=kOutput, calls=%fused_computation.42 | convolution fusion | flops 4297064448 | bytes 10485760 | tf_op jit(solution)/shard_map/dot_general | solution.py:110
  333.8 52.7 %reduce-scatter.2.cloned.1.call-done = bf16[8,128,512]{2,1,0:T(8,128)(2,1)} async-done(((bf16[8,128,2048]{2,1,0:T(8,128)(2,1)}), bf16[8,128,512]{2,1,0:T(8,128)(2,1)}) %reduce-scatter.2.cloned.1.call-update) | async-done | bytes 1048592 | tf_op jit(solution)/shard_map/reduce_scatter | solution.py:115
  386.5 4.6 %all-to-all-start.1 = ((bf16[8,128,512]{2,1,0:T(8,128)(2,1)}), bf16[8,128,512]{2,1,0:T(8,128)(2,1)S(1)}, u32[]{:S(2)}, u32[]{:S(2)}) async-start(bf16[8,128,512]{2,1,0:T(8,128)(2,1)} %reduce-scatter.2.cloned.1.call-done), calls=%async_computation.2 | async-start | bytes 2097152 | tf_op jit(solution)/shard_map/all_to_all | solution.py:119
  391.4 26.3 %all-to-all-done.1 = bf16[8,128,512]{2,1,0:T(8,128)(2,1)S(1)} async-done(((bf16[8,128,512]{2,1,0:T(8,128)(2,1)}), bf16[8,128,512]{2,1,0:T(8,128)(2,1)S(1)}, u32[]{:S(2)}, u32[]{:S(2)}) %all-to-all-start.1) | async-done | bytes 1048608 | tf_op jit(solution)/shard_map/all_to_all | solution.py:119
  417.7 2.6 gather_fusion.1
  420.3 1.7 reshape.117
  422.0 1.3 multiply_reduce_fusion.1
  423.3 1.8 add_convert_fusion.1
  (58 shorter events, 2.3 us)
Async XLA Ops:
  6.5 91.0 %copy-start = (bf16[512,2048]{1,0:T(8,128)(2,1)S(1)}, bf16[512,2048]{1,0:T(8,128)(2,1)}, u32[]{:S(2)}) copy-start(bf16[512,2048]{1,0:T(8,128)(2,1)} %param.17) | copy-start | bytes 6291460
  6.5 35.8 %all-gather.4.cloned.1.call-start = ((), (), s32[]{:S(2)}) async-start(), calls=%async_computation.3 | async-start | bytes 2359296 | tf_op jit(solution)/shard_map/all_gather | solution.py:78
  8.5 65.0 %all-gather.6.cloned.1.call-start = ((), (), s32[]{:S(2)}) async-start(), calls=%async_computation.4 | async-start | bytes 2359296 | tf_op jit(solution)/shard_map/all_gather | solution.py:77
  10.4 211.6 %all-reduce.3.cloned.1.call-start = ((), (), s32[]{:S(2)}) async-start(), calls=%async_computation.5 | async-start | bytes 2097152 | tf_op jit(solution)/shard_map/psum | solution.py:84
  97.4 1.9 copy-start.4
  97.5 124.5 %copy-start.1 = (bf16[256,2048]{1,0:T(8,128)(2,1)S(1)}, bf16[256,2048]{1,0:T(8,128)(2,1)}, u32[]{:S(2)}) copy-start(bf16[256,2048]{1,0:T(8,128)(2,1)} %param.13) | copy-start | bytes 3145732
  97.5 127.5 %copy-start.3 = (f32[2048]{0:T(1024)S(1)}, f32[2048]{0:T(1024)}, u32[]{:S(2)}) copy-start(f32[2048]{0:T(1024)} %param.18) | copy-start | bytes 24580
  99.3 215.3 %all-gather.8.cloned.1.call-start = ((), (), s32[]{:S(2)}) async-start(), calls=%async_computation.6 | async-start | bytes 5242880 | tf_op jit(solution)/shard_map/all_gather | solution.py:104
  222.0 3.0 copy-start.2
  264.1 122.4 %reduce-scatter.2.cloned.1.call-start = ((), (), s32[]{:S(2)}) async-start(), calls=%async_computation.7 | async-start | bytes 5242880 | tf_op jit(solution)/shard_map/reduce_scatter | solution.py:115
  314.6 7.7 %copy-start.6 = (bf16[1,2048,1024]{2,1,0:T(8,128)(2,1)S(1)}, bf16[1,2048,1024]{2,1,0:T(8,128)(2,1)}, u32[]{:S(2)}) copy-start(bf16[1,2048,1024]{2,1,0:T(8,128)(2,1)} %param.21) | copy-start | bytes 12582916
  314.6 7.7 %copy-start.8 = (bf16[8,128,2048]{2,1,0:T(8,128)(2,1)S(1)}, bf16[8,128,2048]{2,1,0:T(8,128)(2,1)}, u32[]{:S(2)}) copy-start(bf16[8,128,2048]{2,1,0:T(8,128)(2,1)} %all-gather.8.cloned.1.call-done) | copy-start | bytes 12582916
  322.3 5.4 %copy-start.7 = (bf16[1,1024,2048]{2,1,0:T(8,128)(2,1)S(1)}, bf16[1,1024,2048]{2,1,0:T(8,128)(2,1)}, u32[]{:S(2)}) copy-start(bf16[1,1024,2048]{2,1,0:T(8,128)(2,1)} %param.23) | copy-start | bytes 12582916
  333.7 57.4 %copy-start.5 = (f32[256,2]{0,1:T(2,128)S(1)}, f32[256,2]{0,1:T(2,128)}, u32[]{:S(2)}) copy-start(f32[256,2]{0,1:T(2,128)} %param.20) | copy-start | bytes 6148
  386.5 31.2 %all-to-all-start.1 = ((bf16[8,128,512]{2,1,0:T(8,128)(2,1)}), bf16[8,128,512]{2,1,0:T(8,128)(2,1)S(1)}, u32[]{:S(2)}, u32[]{:S(2)}) async-start(bf16[8,128,512]{2,1,0:T(8,128)(2,1)} %reduce-scatter.2.cloned.1.call-done), calls=%async_computation.2 | async-start | bytes 2097152 | tf_op jit(solution)/shard_map/all_to_all | solution.py:119
Sparse Core Ops, SparseCore 0:
  8.9 33.3 all-gather.3
  43.9 29.6 all-gather.5
  99.4 122.5 all-reduce.2
  264.2 50.3 all-gather.7
  333.9 52.5 reduce-scatter.1
where the time goes:
time: 432 us
  waiting for transfers between devices  309 us (72%)
  blocking collectives  31.1 us (7%)
  matrix products  25 us (6%)
  other arithmetic  24.9 us (6%)
  local copies, waits for them, and re-layouts  23 us (5%)
  between operations  13.4 us (3%)
  starting transfers between devices  4.78 us (1%)
    psum x1, waiting for transfers between devices, shards(): lax.psum(partial_value, 'tp').astype(jnp.float32).astype(jnp.bfloat16)  118 us
    reduce_scatter x1, waiting for transfers between devices, shards(): lax.psum_scatter(expert_part, 'tp', scatter_dimension=2, tiled=True)  52.7 us
    all_gather x1, waiting for transfers between devices, shards(): arrived = lax.all_gather(arrived, 'tp', axis=2, tiled=True)  50.5 us
    all_gather x1, waiting for transfers between devices, shards(): lax.all_gather(keys, 'sp', axis=0, tiled=True)  31.2 us
    all_to_all x1, blocking collectives, shards(): lax.all_to_all(own_part, 'sp', split_axis=0, concat_axis=0, tiled=True)  31.1 us
    all_gather x1, waiting for transfers between devices, shards(): lax.all_gather(values, 'sp', axis=0, tiled=True)  30.8 us
    all_to_all x1, waiting for transfers between devices, shards(): lax.all_to_all(summed, 'sp', split_axis=0, concat_axis=0, tiled=True)  26.3 us
    another operation x4, other arithmetic  11.3 us
  transfers between devices with their start and end apart: 6, of which 6 were waited for; matrix products, arithmetic and copies ran while one was open for 2% of the time, Pallas kernels for 0%

commit v1 on v0

--- a/solution.py
+++ b/solution.py
@@ -101,7 +101,7 @@
     column_start = lax.axis_index("tp") * col_count
     own_part = lax.dynamic_slice_in_dim(outgoing, column_start, col_count, 2)
     arrived = lax.all_to_all(own_part, "sp", split_axis=0, concat_axis=0, tiled=True)
-    arrived = lax.all_gather(arrived, "tp", axis=2, tiled=True)
+    arrived = jnp.concatenate(lax.all_gather(arrived, "tp"), axis=2)
     slot_rows = arrived.reshape(-1, width)
     gate_act = jnp.dot(slot_rows, gate_weight[0], preferred_element_type=jnp.float32)
     up_act = jnp.dot(slot_rows, up_weight[0], preferred_element_type=jnp.float32)

time: 432 us -> 447 us (1.035)
  local copies, waits for them, and re-layouts: 23 us -> 30.5 us
  matrix products: 25 us -> 32.2 us
    dot_general x1, matrix products: 6.07 us -> 16.3 us  [shards(): jnp.dot(hidden, down_weight[0], preferred_element_type=jnp.float32)]
    reshape x0 -> x1, local copies, waits for them, and re-layouts: none -> 7.51 us  [shards(): arrived = jnp.concatenate(lax.all_gather(arrived, 'tp'), axis=2)]
    dot_general x1 -> x0, matrix products: 5.35 us -> none  [shards(): jnp.dot(slot_rows, gate_weight[0], preferred_element_type=jnp.float32)]
where the time goes in v1:
time: 447 us
  waiting for transfers between devices  310 us (69%)
  matrix products  32.2 us (7%)
  blocking collectives  31.1 us (7%)
  local copies, waits for them, and re-layouts  30.5 us (7%)
  other arithmetic  24.9 us (6%)
  between operations  13.4 us (3%)
  starting transfers between devices  4.78 us (1%)
    psum x1, waiting for transfers between devices, shards(): lax.psum(partial_value, 'tp').astype(jnp.float32).astype(jnp.bfloat16)  118 us
    reduce_scatter x1, waiting for transfers between devices, shards(): lax.psum_scatter(expert_part, 'tp', scatter_dimension=2, tiled=True)  52.8 us
    all_gather x1, waiting for transfers between devices, shards(): arrived = jnp.concatenate(lax.all_gather(arrived, 'tp'), axis=2)  50.6 us
    all_gather x1, waiting for transfers between devices, shards(): lax.all_gather(keys, 'sp', axis=0, tiled=True)  31.2 us
    all_to_all x1, blocking collectives, shards(): lax.all_to_all(own_part, 'sp', split_axis=0, concat_axis=0, tiled=True)  31.1 us
    all_gather x1, waiting for transfers between devices, shards(): lax.all_gather(values, 'sp', axis=0, tiled=True)  30.8 us
    all_to_all x1, waiting for transfers between devices, shards(): lax.all_to_all(summed, 'sp', split_axis=0, concat_axis=0, tiled=True)  26.3 us
    dot_general x1, matrix products, shards(): jnp.dot(hidden, down_weight[0], preferred_element_type=jnp.float32)  16.3 us
  transfers between devices with their start and end apart: 6, of which 6 were waited for; matrix products, arithmetic and copies ran while one was open for 2% of the time, Pallas kernels for 0%

profile of v1, /device:TPU:0, one launch (start us, length us, event | category | flops | bytes accessed | tf_op | source)
XLA Modules:
  0.0 446.6 jit_solution(4780756000065381146)
XLA Ops:
  6.5 1.9 copy.43
  8.6 1.8 copy.44
  10.4 1.1 copy.45
  11.5 30.8 %all-gather.5.cloned.1.call-done = bf16[2048,512]{0,1:T(8,128)(2,1)} async-done(((bf16[256,512]{0,1:T(8,128)(2,1)}), bf16[2048,512]{0,1:T(8,128)(2,1)}) %all-gather.5.cloned.1.call-update) | async-done | bytes 2097168 | tf_op jit(solution)/shard_map/all_gather | solution.py:78
  42.3 31.2 %all-gather.7.cloned.1.call-done = bf16[2048,512]{0,1:T(8,128)(2,1)} async-done(((bf16[256,512]{0,1:T(8,128)(2,1)}), bf16[2048,512]{0,1:T(8,128)(2,1)}) %all-gather.7.cloned.1.call-update) | async-done | bytes 2097168 | tf_op jit(solution)/shard_map/all_gather | solution.py:77
  73.6 23.8 %while.15 = (s32[]{:T(128)}, f32[256,8,64]{0,2,1:T(8,128)S(1)}, f32[8,256]{1,0:T(8,128)S(1)}, s32[]{:T(128)}, s32[]{:T(128)}, /*index=5*/bf16[2048,512]{0,1:T(8,...) while((s32[]{:T(128)}, f32[256,8,64]{0,2,1:T(8,128)S(1)}, ...), condition=%wide.region_4.5_spmd.clone, body=%wide.region_0.4_spmd.clone.sunk | while | flops 436501248 | bytes 51206344 | solution.py:49
  73.6 1.3 constant_dynamic-slice_fusion.4
  75.1 3.6 fusion.73
  78.7 10.1 %fusion.74 = f32[8,256,4,128]{1,0,3,2:T(8,128)S(1)} fusion(f32[8,256,4,128]{1,3,2,0:T(8,128)S(1)} %bitcast.115), kind=kOutput, calls=%fused_computation.22.clone.1 | output fusion | flops 133169152 | bytes 8388608 | tf_op jit(solution)/shard_map/reduce-window.6
  89.2 1.4 copy.70
  90.6 6.3 %fusion.76 = bf16[8,256,512]{1,2,0:T(8,128)(2,1)S(1)} fusion(f32[8,256,4,128]{1,3,2,0:T(8,128)S(1)} %copy.70, f32[8,512,256]{2,1,0:T(8,128)S(1)} %get-tuple-element.219, f32[8,256]{1,0:T(8,128)S(1)} %get-tuple-element.236, pred[256,512]{0,1:T(8,128)(4,1)S(1)} %broadcast_compare_fusion.2), kind=kLoop, calls=%fused_computation.10.clone.1 | loop fusion | flops 23068672 | bytes 10625024 | tf_op jit(solution)/shard_map/while/body/convert_element_type | solution.py:37
  96.9 0.5 fusion.77
  97.5 1.8 convolution_convert_fusion
  100.1 1.1 reduce-window.24
  101.6 2.6 scatter_custom_fusion
  104.3 117.7 %all-reduce.3.cloned.1.call-done = bf16[256,2048]{1,0:T(8,128)(2,1)} async-done(((bf16[256,2048]{1,0:T(8,128)(2,1)}), bf16[256,2048]{1,0:T(8,128)(2,1)}) %all-reduce.3.cloned.1.call-update) | async-done | bytes 1048592 | tf_op jit(solution)/shard_map/psum | solution.py:84
  222.0 3.0 fusion.41
  225.0 0.5 multiply_convert_fusion.2
  225.6 6.0 %gather_fusion = bf16[1024,2048]{1,0:T(8,128)(2,1)} fusion(bf16[257,2048]{1,0:T(8,128)(2,1)S(1)} %concatenate.3, s32[1024]{0:T(1024)S(1)} %fusion.45), kind=kCustom, calls=%fused_computation | custom fusion | bytes 8392704 | tf_op jit(solution)/shard_map/gather | solution.py:99
  231.7 1.3 constant_dynamic-slice_fusion.2
  233.0 31.1 %all_to_all.10 = bf16[8,128,512]{2,1,0:T(8,128)(2,1)} all-to-all(bf16[8,128,512]{2,1,0:T(8,128)(2,1)S(1)} %constant_dynamic-slice_fusion.2), channel_id=1, replica_groups=mesh['sp'=8,'tp'=4] {'sp'}, dimensions={0} | all-to-all | bytes 2097152 | tf_op jit(solution)/shard_map/all_to_all | solution.py:103
  264.1 50.6 %all-gather.9.cloned.1.call-done = bf16[32,128,512]{2,1,0:T(8,128)(2,1)} async-done(((bf16[8,128,512]{2,1,0:T(8,128)(2,1)}), bf16[32,128,512]{2,1,0:T(8,128)(2,1)}) %all-gather.9.cloned.1.call-update) | async-done | bytes 4194320 | tf_op jit(solution)/shard_map/all_gather | solution.py:104
  314.8 7.5 %copy.49 = bf16[8,128,4,512]{1,0,3,2:T(8,128)(2,1)} copy(bf16[8,128,4,512]{3,1,0,2:T(8,128)(2,1)} %bitcast.120) | data formatting | bytes 8388608 | tf_op jit(solution)/shard_map/reshape | solution.py:104
  322.3 10.0 %fusion.19 = f32[1024,1024]{1,0:T(8,128)} fusion(bf16[1,2048,1024]{2,1,0:T(8,128)(2,1)} %param.22, bf16[256,8,8,128]{3,2,1,0:T(8,128)(2,1)} %bitcast.122), kind=kOutput, calls=%fused_computation.35 | convolution fusion | flops 4294967296 | bytes 12582912 | tf_op jit(solution)/shard_map/dot_general | solution.py:107
  332.3 16.3 %fusion.27 = bf16[1024,2048]{1,0:T(8,128)(2,1)} fusion(bf16[1,1024,2048]{2,1,0:T(8,128)(2,1)} %param.23, f32[1024,1024]{1,0:T(8,128)} %fusion.19, bf16[1,2048,1024]{2,1,0:T(8,128)(2,1)} %param.21, bf16[256,8,8,128]{3,2,1,0:T(8,128)(2,1)} %bitcast.123), kind=kOutput, calls=%fused_computation.44 | convolution fusion | flops 8598323200 | bytes 20971520 | tf_op jit(solution)/shard_map/dot_general | solution.py:110
  348.6 52.8 %reduce-scatter.2.cloned.1.call-done = bf16[8,128,512]{2,1,0:T(8,128)(2,1)} async-done(((bf16[8,128,2048]{2,1,0:T(8,128)(2,1)}), bf16[8,128,512]{2,1,0:T(8,128)(2,1)}) %reduce-scatter.2.cloned.1.call-update) | async-done | bytes 1048592 | tf_op jit(solution)/shard_map/reduce_scatter | solution.py:115
  401.4 4.6 %all-to-all-start.1 = ((bf16[8,128,512]{2,1,0:T(8,128)(2,1)}), bf16[8,128,512]{2,1,0:T(8,128)(2,1)S(1)}, u32[]{:S(2)}, u32[]{:S(2)}) async-start(bf16[8,128,512]{2,1,0:T(8,128)(2,1)} %reduce-scatter.2.cloned.1.call-done), calls=%async_computation.2 | async-start | bytes 2097152 | tf_op jit(solution)/shard_map/all_to_all | solution.py:119
  406.3 26.3 %all-to-all-done.1 = bf16[8,128,512]{2,1,0:T(8,128)(2,1)S(1)} async-done(((bf16[8,128,512]{2,1,0:T(8,128)(2,1)}), bf16[8,128,512]{2,1,0:T(8,128)(2,1)S(1)}, u32[]{:S(2)}, u32[]{:S(2)}) %all-to-all-start.1) | async-done | bytes 1048608 | tf_op jit(solution)/shard_map/all_to_all | solution.py:119
  432.6 2.6 gather_fusion.1
  435.2 1.7 reshape.117
  436.9 1.3 multiply_reduce_fusion.1
  438.2 1.8 add_convert_fusion.1
  (52 shorter events, 2.3 us)
Async XLA Ops:
  6.5 91.0 %copy-start = (bf16[512,2048]{1,0:T(8,128)(2,1)S(1)}, bf16[512,2048]{1,0:T(8,128)(2,1)}, u32[]{:S(2)}) copy-start(bf16[512,2048]{1,0:T(8,128)(2,1)} %param.17) | copy-start | bytes 6291460
  6.5 35.8 %all-gather.5.cloned.1.call-start = ((), (), s32[]{:S(2)}) async-start(), calls=%async_computation.3 | async-start | bytes 2359296 | tf_op jit(solution)/shard_map/all_gather | solution.py:78
  8.5 65.0 %all-gather.7.cloned.1.call-start = ((), (), s32[]{:S(2)}) async-start(), calls=%async_computation.4 | async-start | bytes 2359296 | tf_op jit(solution)/shard_map/all_gather | solution.py:77
  10.4 211.6 %all-reduce.3.cloned.1.call-start = ((), (), s32[]{:S(2)}) async-start(), calls=%async_computation.5 | async-start | bytes 2097152 | tf_op jit(solution)/shard_map/psum | solution.py:84
  97.4 1.9 copy-start.4
  97.5 124.5 %copy-start.1 = (bf16[256,2048]{1,0:T(8,128)(2,1)S(1)}, bf16[256,2048]{1,0:T(8,128)(2,1)}, u32[]{:S(2)}) copy-start(bf16[256,2048]{1,0:T(8,128)(2,1)} %param.13) | copy-start | bytes 3145732
  97.5 127.5 %copy-start.3 = (f32[2048]{0:T(1024)S(1)}, f32[2048]{0:T(1024)}, u32[]{:S(2)}) copy-start(f32[2048]{0:T(1024)} %param.18) | copy-start | bytes 24580
  99.3 215.5 %all-gather.9.cloned.1.call-start = ((), (), s32[]{:S(2)}) async-start(), calls=%async_computation.7 | async-start | bytes 5242880 | tf_op jit(solution)/shard_map/all_gather | solution.py:104
  222.0 3.0 copy-start.2
  264.1 137.3 %reduce-scatter.2.cloned.1.call-start = ((), (), s32[]{:S(2)}) async-start(), calls=%async_computation.6 | async-start | bytes 5242880 | tf_op jit(solution)/shard_map/reduce_scatter | solution.py:115
  348.6 57.4 %copy-start.5 = (f32[256,2]{0,1:T(2,128)S(1)}, f32[256,2]{0,1:T(2,128)}, u32[]{:S(2)}) copy-start(f32[256,2]{0,1:T(2,128)} %param.20) | copy-start | bytes 6148
  401.4 31.2 %all-to-all-start.1 = ((bf16[8,128,512]{2,1,0:T(8,128)(2,1)}), bf16[8,128,512]{2,1,0:T(8,128)(2,1)S(1)}, u32[]{:S(2)}, u32[]{:S(2)}) async-start(bf16[8,128,512]{2,1,0:T(8,128)(2,1)} %reduce-scatter.2.cloned.1.call-done), calls=%async_computation.2 | async-start | bytes 2097152 | tf_op jit(solution)/shard_map/all_to_all | solution.py:119
Sparse Core Ops, SparseCore 0:
  8.9 33.3 all-gather.4
  43.9 29.6 all-gather.6
  99.4 122.5 all-reduce.2
  264.2 50.5 all-gather.8
  348.7 52.5 reduce-scatter.1
